TPU v7x, 32 devices: a whole 2x2x4 slice. The times are simulated.
32 devices in a mesh: sp: 8 (over z, y), tp: 4 (over x, core).
Axes of the slice: x: 2, y: 2, z: 4, core: 2. Of those that a mesh axis runs over, the one named last changes fastest.
Arguments:
- tokens: bfloat16 [2048, 1024], P(('sp', 'tp')), may hold values from -7.5 to 7.5, as said below
- query_weight: bfloat16 [1024, 2048], P('sp', 'tp'), may hold values from -0.1875 to 0.1875
- key_weight: bfloat16 [1024, 2048], P('sp', 'tp'), may hold values from -0.1875 to 0.1875
- value_weight: bfloat16 [1024, 2048], P('sp', 'tp'), may hold values from -0.1875 to 0.1875
- gate_weight: bfloat16 [1024, 16], P('sp', 'tp'), may hold values from -0.1875 to 0.1875
- forget_bias: float32 [16], P('tp'), may hold values from 0 to 2
- out_weight: bfloat16 [2048, 1024], P('tp', 'sp'), may hold values from -0.125 to 0.125
- out_gain: float32 [1024], replicated, may hold values from 0.5 to 1.5
Outputs:
- mixed: bfloat16 [2048, 1024], P(('sp', 'tp'))
Inputs may be any that keep to these rules, and one draw needn't show every extreme that they name: `tokens`: each entry is a bounded noise value (at most 6 in size) plus an offset in -1.5 to 1.5 shared by the 256 rows of one index of sp, so every entry lies within -7.5 and 7.5.
All inputs are finite; a program needn't handle non-finite values.
Results may differ from a plain program's by a relative error of at most 0.006.
Values may be sent and summed in bfloat16 or wider, within the bound.
A program may use at most 128 MiB of HBM per device.

v0:
```python
import math
import jax
import jax.numpy as jnp
from jax import lax
from jax.sharding import PartitionSpec as P


def on_whole(shard, axis, dim, block):
    whole = lax.all_gather(shard, axis, axis=dim, tiled=True)
    return block(whole, jnp.int32(0))


def over_all(shard, axis, dim, absorb, state):
    everything = jax.tree.map(lambda a: lax.all_gather(a, axis, axis=dim, tiled=True), shard)
    return absorb(state, everything, jnp.int32(0))


def own_rows(product, width, axis):
    everything = product(jnp.int32(0), lax.axis_size(axis) * width)
    own = lax.psum_scatter(everything, axis, scatter_dimension=0, tiled=True)
    return own


def on_device(
    tokens, query_weight, key_weight, value_weight, gate_weight, forget_bias, out_weight, out_gain
):
    width = query_weight.shape[1]
    heads = gate_weight.shape[1]
    head_size = width // heads
    whole_q = lax.all_gather(query_weight, "sp", axis=0, tiled=True)
    whole_k = lax.all_gather(key_weight, "sp", axis=0, tiled=True)
    whole_v = lax.all_gather(value_weight, "sp", axis=0, tiled=True)
    whole_g = lax.all_gather(gate_weight, "sp", axis=0, tiled=True)
    joined = jnp.concatenate([whole_q, whole_k, whole_v, whole_g], axis=1)

    def project(piece, start):
        return jnp.dot(piece, joined, preferred_element_type=jnp.float32)

    projected = on_whole(tokens, "tp", 0, project)
    block = projected.shape[0]
    queries = projected[:, :width].astype(jnp.bfloat16).reshape(block, heads, head_size)
    keys = projected[:, width : 2 * width].astype(jnp.bfloat16).reshape(block, heads, head_size)
    values = (
        projected[:, 2 * width : 3 * width].astype(jnp.bfloat16).reshape(block, heads, head_size)
    )
    seq_len = block * lax.axis_size("sp")
    log_gate = jax.nn.log_sigmoid(projected[:, 3 * width :] + forget_bias + math.log(seq_len))
    gates_all = lax.all_gather(log_gate, "sp", axis=0, tiled=True)
    cumulative = jnp.cumsum(gates_all, axis=0)
    first = lax.axis_index("sp") * block
    query_cum = lax.dynamic_slice_in_dim(cumulative, first, block, 0)
    query_pos = first + jnp.arange(block, dtype=jnp.int32)
    scale = head_size ** (-0.5)

    def update(carry, piece, start):
        run_max, run_sum, run_acc = carry
        key_piece, value_piece = piece
        length = key_piece.shape[0]
        key_cum = lax.dynamic_slice_in_dim(cumulative, start, length, 0)
        logits = (
            jnp.einsum("qhd,khd->hqk", queries, key_piece, preferred_element_type=jnp.float32)
            * scale
        )
        logits = logits + query_cum.T[:, :, None] - key_cum.T[:, None, :]
        key_pos = start + jnp.arange(length, dtype=jnp.int32)
        allowed = (key_pos[None, :] <= query_pos[:, None])[None]
        logits = jnp.where(allowed, logits, -1e30)
        new_max = jnp.maximum(run_max, jnp.max(logits, axis=-1))
        probs = jnp.where(allowed, jnp.exp(logits - new_max[..., None]), 0.0)
        factor = jnp.exp(run_max - new_max)
        new_sum = run_sum * factor + jnp.sum(probs, axis=-1)
        new_acc = run_acc * factor[..., None] + jnp.einsum(
            "hqk,khd->hqd", probs, value_piece.astype(jnp.float32)
        )
        return (new_max, new_sum, new_acc)

    def attend(carry, piece, start):
        return lax.cond(
            start > first + block - 1,
            lambda state: state,
            lambda state: update(state, piece, start),
            carry,
        )

    initial = (
        jnp.full((heads, block), -1e30, jnp.float32),
        jnp.zeros((heads, block), jnp.float32),
        jnp.zeros((heads, block, head_size), jnp.float32),
    )
    run_max, run_sum, run_acc = over_all((keys, values), "sp", 0, attend, initial)
    attended = (
        (run_acc / run_sum[..., None]).transpose(1, 0, 2).reshape(block, width).astype(jnp.bfloat16)
    )
    out_full = lax.all_gather(out_weight, "sp", axis=1, tiled=True)
    rows = tokens.shape[0]

    def term(start, count):
        return jnp.dot(
            lax.dynamic_slice_in_dim(attended, start, count, 0),
            out_full,
            preferred_element_type=jnp.float32,
        )

    summed = own_rows(term, rows, "tp")
    normed = summed * lax.rsqrt(jnp.mean(summed * summed, axis=-1, keepdims=True) + 1e-06)
    return (normed * out_gain).astype(jnp.bfloat16)


def solution(mesh):
    placed = (
        P(("sp", "tp"), None),
        P("sp", "tp"),
        P("sp", "tp"),
        P("sp", "tp"),
        P("sp", "tp"),
        P("tp"),
        P("tp", "sp"),
        P(),
    )
    return jax.shard_map(
        on_device, mesh=mesh, in_specs=placed, out_specs=P(("sp", "tp"), None), check_vma=False
    )
```

profile of v0, /device:TPU:0, one launch (start us, length us, event | category | flops | bytes accessed | tf_op | source)
XLA Modules:
  0.0 312.7 jit_solution(10969626571004091959)
XLA Ops:
  6.5 0.0 all-gather.11.cloned.1.call-start
  6.5 0.7 all-gather.11.cloned.1.call-update
  7.3 0.0 all-gather.9.cloned.1.call-start
  7.3 0.7 all-gather.9.cloned.1.call-update
  8.0 0.0 all-gather.7.cloned.1.call-start
  8.1 0.7 all-gather.7.cloned.1.call-update
  8.7 0.0 all-gather.13.cloned.1.call-start
  8.8 22.6 %all_gather.30 = bf16[1024,4]{0,1:T(4,128)(2,1)S(1)} all-gather(bf16[128,4]{0,1:T(4,128)(2,1)} %param.14), channel_id=1, replica_groups=mesh['sp'=8,'tp'=4] {'sp'}, dimensions={0}, use_global_device_ids=true | all-gather | bytes 9216 | tf_op jit(solution)/shard_map/all_gather | solution.py:33
  31.4 0.2 copy.14
  31.6 7.4 %all_gather.31 = bf16[256,1024]{1,0:T(8,128)(2,1)S(1)} all-gather(bf16[64,1024]{1,0:T(8,128)(2,1)} %param.10), channel_id=1, replica_groups=mesh['sp'=8,'tp'=4] {'tp'}, dimensions={0}, use_global_device_ids=true | all-gather | bytes 655360 | tf_op jit(solution)/shard_map/all_gather | solution.py:9
  38.9 0.0 copy-start.1
  39.0 13.5 %all-gather.11.cloned.1.call-done = bf16[1024,512]{1,0:T(8,128)(2,1)} async-done(((bf16[128,512]{1,0:T(8,128)(2,1)}), bf16[1024,512]{1,0:T(8,128)(2,1)}) %all-gather.11.cloned.1.call-update) | async-done | bytes 1048592 | tf_op jit(solution)/shard_map/all_gather | solution.py:32
  52.5 41.1 %all-gather.9.cloned.1.call-done = bf16[1024,512]{1,0:T(8,128)(2,1)} async-done(((bf16[128,512]{1,0:T(8,128)(2,1)}), bf16[1024,512]{1,0:T(8,128)(2,1)}) %all-gather.9.cloned.1.call-update) | async-done | bytes 1048592 | tf_op jit(solution)/shard_map/all_gather | solution.py:31
  93.6 41.2 %all-gather.7.cloned.1.call-done = bf16[1024,512]{1,0:T(8,128)(2,1)} async-done(((bf16[128,512]{1,0:T(8,128)(2,1)}), bf16[1024,512]{1,0:T(8,128)(2,1)}) %all-gather.7.cloned.1.call-update) | async-done | bytes 1048592 | tf_op jit(solution)/shard_map/all_gather | solution.py:30
  134.8 2.9 fusion.32
  137.8 0.9 copy.15
  138.6 0.0 all-gather.13.cloned.1.call-update
  138.7 0.0 all-gather.15.cloned.1.call-start
  138.7 0.8 copy.16
  139.6 0.0 all-gather.15.cloned.1.call-update
  139.6 0.0 all-gather.17.cloned.1.call-start
  139.6 0.5 all-gather.17.cloned.1.call-update
  140.2 0.0 reduce-scatter.2.cloned.1.call-start
  140.2 0.0 copy-done.1
  140.2 0.1 fusion.26
  140.3 31.0 %all_gather.33 = f32[2048,4]{0,1:T(4,128)S(1)} all-gather(f32[256,4]{0,1:T(4,128)S(1)} %fusion.26), channel_id=1, replica_groups=mesh['sp'=8,'tp'=4] {'sp'}, dimensions={0}, use_global_device_ids=true | all-gather | bytes 36864 | tf_op jit(solution)/shard_map/all_gather | solution.py:48
  171.3 1.1 reduce-window.6
  172.4 0.2 slice_reduce_fusion
  172.6 0.2 reduce-window.9
  172.8 0.1 add_bitcast_fusion
  172.9 13.9 %all-gather.13.cloned.1.call-done = bf16[2048,4,128]{2,0,1:T(8,128)(2,1)} async-done(((bf16[256,4,128]{2,0,1:T(8,128)(2,1)}), bf16[2048,4,128]{2,0,1:T(8,128)(2,1)}) %all-gather.13.cloned.1.call-update) | async-done | bytes 2097168 | tf_op jit(solution)/shard_map/all_gather | solution.py:14
  186.9 49.7 %all-gather.15.cloned.1.call-done = bf16[2048,4,128]{2,0,1:T(8,128)(2,1)} async-done(((bf16[256,4,128]{2,0,1:T(8,128)(2,1)}), bf16[2048,4,128]{2,0,1:T(8,128)(2,1)}) %all-gather.15.cloned.1.call-update) | async-done | bytes 2097168 | tf_op jit(solution)/shard_map/all_gather | solution.py:14
  236.6 0.0 copy-start
  236.6 11.8 %conditional.1 = (f32[4,256]{1,0:T(4,128)S(1)}, f32[4,256,128]{1,2,0:T(8,128)S(1)}) conditional(s32[]{:T(128)} %convert_element_type.19, (s32[]{:T(128)}, s32[256]{0:T(256)S(1)}, bf16[256,1540]{0,1:T(8,128)(2,1)S(1)}, bf16[2048,4,128]{2,0,1:T(8,128)(2,1)}, f32[256,4]{0,1:T(4,128)S(1)}, /*index=5*/f32[2048,4]{0,1:T(4,128)S(1)}, ...), branch_computations={%region_2.5_spmd, %region_5.6_spmd} | conditional | flops 1112149248 | bytes 42363952 | solution.py:78
  236.6 0.4 iota_compare_fusion
  237.0 0.0 copy-start.2
  237.0 4.6 %fusion.2 = (f32[4,256]{1,0:T(4,128)S(1)}, f32[4,256,2048]{2,1,0:T(8,128)S(1)}) fusion(f32[4,2048]{1,0:T(4,128)S(1)} %bitcast.40, f32[4,256]{1,0:T(4,128)S(1)} %bitcast.45, pred[256,2048]{1,0:T(8,128)(4,1)S(1)} %iota_compare_fusion, bf16[256,4,128]{0,2,1:T(8,128)(2,1)S(1)} %bitcast.37, bf16[2048,4,128]{2,0,1:T(8,128)(2,1)} %get-tuple-element.25), kind=kOutput, calls=%fused_computation.4 | convolution fusion | flops 547355648 | bytes 11313152 | tf_op jit(solution)/shard_map/cond/branch_0_fun/qhd,khd->hqk/dot_general | solution.py:61
  241.7 3.2 %fusion.1 = f32[4,256]{1,0:T(4,128)S(1)} fusion(f32[4,256,2048]{2,1,0:T(8,128)S(1)} %get-tuple-element.45, f32[4,256]{1,0:T(4,128)S(1)} %broadcast_maximum_fusion, f32[4,2048]{1,0:T(4,128)S(1)} %bitcast.41, f32[4,256]{1,0:T(4,128)S(1)} %bitcast.46, pred[256,2048]{1,0:T(8,128)(4,1)S(1)} %iota_compare_fusion), kind=kLoop, calls=%fused_computation.3 | loop fusion | flops 14679040 | bytes 8957952 | tf_op jit(solution)/shard_map/cond/branch_0_fun/reduce_sum | solution.py:71
  244.9 0.0 copy-done.2
  244.9 3.3 %fusion.10 = f32[4,256,128]{2,1,0:T(8,128)S(1)} fusion(bf16[2048,4,128]{2,0,1:T(8,128)(2,1)S(1)} %copy-done.2, f32[4,256,2048]{2,1,0:T(8,128)S(1)} %get-tuple-element.45, f32[4,256]{1,0:T(4,128)S(1)} %broadcast_maximum_fusion, f32[4,2048]{1,0:T(4,128)S(1)} %bitcast.42, f32[4,256]{1,0:T(4,128)S(1)} %bitcast.47, pred[256,2048]{1,0:T(8,128)(4,1)S(1)} %iota_compare_fusion, ...), kind=kOutput, calls=%fused_computation.13 | convolution fusion | flops 549584896 | bytes 11579392 | tf_op jit(solution)/shard_map/cond/branch_0_fun/hqk,khd->hqd/dot_general | solution.py:72
  248.1 0.2 copy.19
  248.4 28.0 %all-gather.17.cloned.1.call-done = bf16[512,1024]{1,0:T(8,128)(2,1)} async-done(((bf16[512,128]{1,0:T(8,128)(2,1)}), bf16[512,1024]{1,0:T(8,128)(2,1)}) %all-gather.17.cloned.1.call-update) | async-done | bytes 1048592 | tf_op jit(solution)/shard_map/all_gather | solution.py:94
  276.5 2.7 fusion.33
  279.1 0.0 reduce-scatter.2.cloned.1.call-update
  279.1 24.0 %reduce-scatter.2.cloned.1.call-done = f32[64,1024]{1,0:T(8,128)} async-done(((f32[256,1024]{1,0:T(8,128)}), f32[64,1024]{1,0:T(8,128)}) %reduce-scatter.2.cloned.1.call-update) | async-done | bytes 262160 | tf_op jit(solution)/shard_map/reduce_scatter | solution.py:20
  303.1 1.1 multiply_reduce_fusion
  304.2 0.0 copy-done
  304.2 1.7 multiply_convert_fusion
  (11 shorter events, 0.2 us)
Async XLA Ops:
  6.5 46.0 %all-gather.11.cloned.1.call-start = ((), (), s32[]{:S(2)}) async-start(), calls=%async_computation.3 | async-start | bytes 1179648 | tf_op jit(solution)/shard_map/all_gather | solution.py:32
  7.3 86.4 %all-gather.9.cloned.1.call-start = ((), (), s32[]{:S(2)}) async-start(), calls=%async_computation.2 | async-start | bytes 1179648 | tf_op jit(solution)/shard_map/all_gather | solution.py:31
  8.0 126.8 %all-gather.7.cloned.1.call-start = ((), (), s32[]{:S(2)}) async-start(), calls=%async_computation.1 | async-start | bytes 1179648 | tf_op jit(solution)/shard_map/all_gather | solution.py:30
  8.7 178.1 %all-gather.13.cloned.1.call-start = ((), (), s32[]{:S(2)}) async-start(), calls=%async_computation.4 | async-start | bytes 2359296 | tf_op jit(solution)/shard_map/all_gather | solution.py:14
  38.9 101.3 %copy-start.1 = (f32[4]{0:T(128)S(1)}, f32[4]{0:T(128)}, u32[]{:S(2)}) copy-start(f32[4]{0:T(128)} %param.15) | copy-start | bytes 52
  138.7 97.9 %all-gather.15.cloned.1.call-start = ((), (), s32[]{:S(2)}) async-start(), calls=%async_computation.5 | async-start | bytes 2359296 | tf_op jit(solution)/shard_map/all_gather | solution.py:14
  139.6 136.9 %all-gather.17.cloned.1.call-start = ((), (), s32[]{:S(2)}) async-start(), calls=%async_computation.6 | async-start | bytes 1179648 | tf_op jit(solution)/shard_map/all_gather | solution.py:94
  140.2 162.9 %reduce-scatter.2.cloned.1.call-start = ((), (), s32[]{:S(2)}) async-start(), calls=%async_computation.7 | async-start | bytes 1310720 | tf_op jit(solution)/shard_map/reduce_scatter | solution.py:20
  236.6 67.6 %copy-start = (f32[1024]{0:T(1024)S(1)}, f32[1024]{0:T(1024)}, u32[]{:S(2)}) copy-start(f32[1024]{0:T(1024)} %param.17) | copy-start | bytes 12292
  237.0 7.9 %copy-start.2 = (bf16[2048,4,128]{2,0,1:T(8,128)(2,1)S(1)}, bf16[2048,4,128]{2,0,1:T(8,128)(2,1)}, u32[]{:S(2)}) copy-start(bf16[2048,4,128]{2,0,1:T(8,128)(2,1)} %get-tuple-element.28) | copy-start | bytes 6291460 | tf_op jit(solution)/shard_map/cond
Sparse Core Ops, SparseCore 0:
  9.5 42.9 all-gather.10
  54.6 38.9 all-gather.8
  95.8 38.9 all-gather.6
  138.8 48.0 all-gather.12
  188.9 47.6 all-gather.14
  238.5 37.9 all-gather.16
  279.3 23.7 reduce-scatter.1
where the time goes:
time: 313 us
  waiting for transfers between devices  214 us (68%)
  blocking collectives  61 us (19%)
  between operations  13.6 us (4%)
  matrix products  13.5 us (4%)
  other arithmetic  7.89 us (3%)
    all_gather x2, waiting for transfers between devices, over_all(): lax.all_gather(a, axis, axis=dim, tiled=True)  63.7 us
    all_gather x1, waiting for transfers between devices, on_device(): whole_q = lax.all_gather(query_weight, 'sp', axis=0, tiled=True)  41.2 us
    all_gather x1, waiting for transfers between devices, on_device(): whole_k = lax.all_gather(key_weight, 'sp', axis=0, tiled=True)  41.1 us
    all_gather x1, blocking collectives, on_device(): gates_all = lax.all_gather(log_gate, 'sp', axis=0, tiled=True)  31 us
    all_gather x1, waiting for transfers between devices, on_device(): out_full = lax.all_gather(out_weight, 'sp', axis=1, tiled=True)  28 us
    reduce_scatter x1, waiting for transfers between devices, own_rows(): own = lax.psum_scatter(everything, axis, scatter_dimension=0, tiled=True)  24 us
    all_gather x1, blocking collectives, on_device(): whole_g = lax.all_gather(gate_weight, 'sp', axis=0, tiled=True)  22.6 us
    all_gather x1, waiting for transfers between devices, on_device(): whole_v = lax.all_gather(value_weight, 'sp', axis=0, tiled=True)  13.5 us
  transfers between devices with their start and end apart: 7, of which 7 were waited for; matrix products, arithmetic and copies ran while one was open for 5% of the time, Pallas kernels for 0%

commit v1 on v0

--- a/solution.py
+++ b/solution.py
@@ -3,6 +3,14 @@
 import jax.numpy as jnp
 from jax import lax
 from jax.sharding import PartitionSpec as P
+
+
+def deliver_sources_all_for(mine_x, u):
+    return jnp.split(
+        jax.lax.all_gather(jnp.concatenate([mine_x, u], 1), "sp", axis=0, tiled=True),
+        [mine_x.shape[1]],
+        1,
+    )
 
 
 def on_whole(shard, axis, dim, block):
@@ -27,8 +35,7 @@
     width = query_weight.shape[1]
     heads = gate_weight.shape[1]
     head_size = width // heads
-    whole_q = lax.all_gather(query_weight, "sp", axis=0, tiled=True)
-    whole_k = lax.all_gather(key_weight, "sp", axis=0, tiled=True)
+    whole_q, whole_k = deliver_sources_all_for(query_weight, key_weight)
     whole_v = lax.all_gather(value_weight, "sp", axis=0, tiled=True)
     whole_g = lax.all_gather(gate_weight, "sp", axis=0, tiled=True)
     joined = jnp.concatenate([whole_q, whole_k, whole_v, whole_g], axis=1)

time: 313 us -> 280 us (0.89)
  waiting for transfers between devices: 214 us -> 180 us
    all_gather x2 -> x1, waiting for transfers between devices: 82.3 us -> 50 us  [deliver_sources_all_for(): jax.lax.all_gather(jnp.concatenate([mine_x, u], 1), 'sp', axis=0, tiled=T...]
  transfers between devices with their start and end apart: 7 -> 6, of which waited for: 7 -> 6; matrix products, arithmetic and copies ran while one was open for 5% -> 6% of each run, Pallas kernels for 0% -> 0%
where the time goes in v1:
time: 280 us
  waiting for transfers between devices  180 us (64%)
  blocking collectives  61 us (22%)
  matrix products  13.6 us (5%)
  between operations  13.6 us (5%)
  other arithmetic  9.58 us (3%)
    all_gather x2, waiting for transfers between devices, over_all(): lax.all_gather(a, axis, axis=dim, tiled=True)  63.3 us
    all_gather x1, waiting for transfers between devices, deliver_sources_all_for(): jax.lax.all_gather(jnp.concatenate([mine_x, u], 1), 'sp', axis=0, tiled=T...  50 us
    all_gather x1, blocking collectives, on_device(): gates_all = lax.all_gather(log_gate, 'sp', axis=0, tiled=True)  31 us
    all_gather x1, waiting for transfers between devices, on_device(): out_full = lax.all_gather(out_weight, 'sp', axis=1, tiled=True)  28 us
    reduce_scatter x1, waiting for transfers between devices, own_rows(): own = lax.psum_scatter(everything, axis, scatter_dimension=0, tiled=True)  24 us
    all_gather x1, blocking collectives, on_device(): whole_g = lax.all_gather(gate_weight, 'sp', axis=0, tiled=True)  22.6 us
    all_gather x1, waiting for transfers between devices, on_device(): whole_v = lax.all_gather(value_weight, 'sp', axis=0, tiled=True)  13.3 us
    all_gather x1, blocking collectives, on_whole(): whole = lax.all_gather(shard, axis, axis=dim, tiled=True)  7.38 us
  transfers between devices with their start and end apart: 6, of which 6 were waited for; matrix products, arithmetic and copies ran while one was open for 6% of the time, Pallas kernels for 0%

profile of v1, /device:TPU:0, one launch (start us, length us, event | category | flops | bytes accessed | tf_op | source)
XLA Modules:
  0.0 280.1 jit_solution(13188903965643147000)
XLA Ops:
  6.5 0.0 all-gather.8.cloned.1.call-start
  6.5 0.7 all-gather.8.cloned.1.call-update
  7.3 0.0 all-gather.6.cloned.1.call-start
  7.3 1.7 pad_maximum_fusion
  9.0 0.0 all-gather.6.cloned.1.call-update
  9.0 0.0 all-gather.10.cloned.1.call-start
  9.1 22.6 %all_gather.26 = bf16[1024,4]{0,1:T(4,128)(2,1)S(1)} all-gather(bf16[128,4]{0,1:T(4,128)(2,1)} %param.14), channel_id=1, replica_groups=mesh['sp'=8,'tp'=4] {'sp'}, dimensions={0}, use_global_device_ids=true | all-gather | bytes 9216 | tf_op jit(solution)/shard_map/all_gather | solution.py:40
  31.6 0.2 copy.14
  31.8 7.4 %all_gather.27 = bf16[256,1024]{1,0:T(8,128)(2,1)S(1)} all-gather(bf16[64,1024]{1,0:T(8,128)(2,1)} %param.10), channel_id=1, replica_groups=mesh['sp'=8,'tp'=4] {'tp'}, dimensions={0}, use_global_device_ids=true | all-gather | bytes 655360 | tf_op jit(solution)/shard_map/all_gather | solution.py:17
  39.2 0.0 copy-start.1
  39.2 13.3 %all-gather.8.cloned.1.call-done = bf16[1024,512]{1,0:T(8,128)(2,1)} async-done(((bf16[128,512]{1,0:T(8,128)(2,1)}), bf16[1024,512]{1,0:T(8,128)(2,1)}) %all-gather.8.cloned.1.call-update) | async-done | bytes 1048592 | tf_op jit(solution)/shard_map/all_gather | solution.py:39
  52.5 50.0 %all-gather.6.cloned.1.call-done = bf16[1024,1024]{1,0:T(8,128)(2,1)} async-done(((bf16[128,1024]{1,0:T(8,128)(2,1)}), bf16[1024,1024]{1,0:T(8,128)(2,1)}) %all-gather.6.cloned.1.call-update) | async-done | bytes 2097168 | tf_op jit(solution)/shard_map/all_gather | solution.py:10
  102.5 3.0 %fusion.30 = (bf16[256,1540]{0,1:T(8,128)(2,1)S(1)}, f32[256,1540]{0,1:T(8,128)S(1)}) fusion(bf16[256,1024]{1,0:T(8,128)(2,1)S(1)} %all_gather.27, bf16[1024,4]{1,0:T(8,128)(2,1)S(1)} %copy.14, bf16[1024,512]{1,0:T(8,128)(2,1)} %all-gather.8.cloned.1.call-done, bf16[1024,1024]{1,0:T(8,128)(2,1)} %all-gather.6.cloned.1.call-done), kind=kOutput, calls=%fused_computation.46 | convolution fusion | flops 817259520 | bytes 6043648 | tf_op jit(solution)/shard_map/dot_general | solution.py:44
  105.5 0.8 copy.15
  106.4 0.0 all-gather.10.cloned.1.call-update
  106.4 0.0 all-gather.12.cloned.1.call-start
  106.4 0.9 copy.16
  107.3 0.0 all-gather.12.cloned.1.call-update
  107.3 0.0 all-gather.14.cloned.1.call-start
  107.4 0.5 all-gather.14.cloned.1.call-update
  107.9 0.0 reduce-scatter.2.cloned.1.call-start
  108.0 0.0 copy-done.1
  108.0 0.1 fusion.24
  108.1 31.0 %all_gather.29 = f32[2048,4]{0,1:T(4,128)S(1)} all-gather(f32[256,4]{0,1:T(4,128)S(1)} %fusion.24), channel_id=1, replica_groups=mesh['sp'=8,'tp'=4] {'sp'}, dimensions={0}, use_global_device_ids=true | all-gather | bytes 36864 | tf_op jit(solution)/shard_map/all_gather | solution.py:55
  139.1 1.1 reduce-window.6
  140.2 0.2 slice_reduce_fusion
  140.4 0.2 reduce-window.9
  140.6 0.1 add_bitcast_fusion
  140.7 13.6 %all-gather.10.cloned.1.call-done = bf16[2048,4,128]{2,0,1:T(8,128)(2,1)} async-done(((bf16[256,4,128]{2,0,1:T(8,128)(2,1)}), bf16[2048,4,128]{2,0,1:T(8,128)(2,1)}) %all-gather.10.cloned.1.call-update) | async-done | bytes 2097168 | tf_op jit(solution)/shard_map/all_gather | solution.py:22
  154.3 49.7 %all-gather.12.cloned.1.call-done = bf16[2048,4,128]{2,0,1:T(8,128)(2,1)} async-done(((bf16[256,4,128]{2,0,1:T(8,128)(2,1)}), bf16[2048,4,128]{2,0,1:T(8,128)(2,1)}) %all-gather.12.cloned.1.call-update) | async-done | bytes 2097168 | tf_op jit(solution)/shard_map/all_gather | solution.py:22
  204.0 0.0 copy-start
  204.0 11.8 %conditional.1 = (f32[4,256]{1,0:T(4,128)S(1)}, f32[4,256,128]{1,2,0:T(8,128)S(1)}) conditional(s32[]{:T(128)} %convert_element_type.19, (s32[]{:T(128)}, s32[256]{0:T(256)S(1)}, bf16[256,1540]{0,1:T(8,128)(2,1)S(1)}, bf16[2048,4,128]{2,0,1:T(8,128)(2,1)}, f32[256,4]{0,1:T(4,128)S(1)}, /*index=5*/f32[2048,4]{0,1:T(4,128)S(1)}, ...), branch_computations={%region_2.5_spmd, %region_5.6_spmd} | conditional | flops 1112149248 | bytes 42363952 | solution.py:85
  204.0 0.4 iota_compare_fusion
  204.4 0.0 copy-start.2
  204.4 4.6 %fusion.2 = (f32[4,256]{1,0:T(4,128)S(1)}, f32[4,256,2048]{2,1,0:T(8,128)S(1)}) fusion(f32[4,2048]{1,0:T(4,128)S(1)} %bitcast.40, f32[4,256]{1,0:T(4,128)S(1)} %bitcast.45, pred[256,2048]{1,0:T(8,128)(4,1)S(1)} %iota_compare_fusion, bf16[256,4,128]{0,2,1:T(8,128)(2,1)S(1)} %bitcast.37, bf16[2048,4,128]{2,0,1:T(8,128)(2,1)} %get-tuple-element.25), kind=kOutput, calls=%fused_computation.4 | convolution fusion | flops 547355648 | bytes 11313152 | tf_op jit(solution)/shard_map/cond/branch_0_fun/qhd,khd->hqk/dot_general | solution.py:68
  209.0 3.2 %fusion.1 = f32[4,256]{1,0:T(4,128)S(1)} fusion(f32[4,256,2048]{2,1,0:T(8,128)S(1)} %get-tuple-element.45, f32[4,256]{1,0:T(4,128)S(1)} %broadcast_maximum_fusion, f32[4,2048]{1,0:T(4,128)S(1)} %bitcast.41, f32[4,256]{1,0:T(4,128)S(1)} %bitcast.46, pred[256,2048]{1,0:T(8,128)(4,1)S(1)} %iota_compare_fusion), kind=kLoop, calls=%fused_computation.3 | loop fusion | flops 14679040 | bytes 8957952 | tf_op jit(solution)/shard_map/cond/branch_0_fun/reduce_sum | solution.py:78
  212.3 0.0 copy-done.2
  212.3 3.3 %fusion.10 = f32[4,256,128]{2,1,0:T(8,128)S(1)} fusion(bf16[2048,4,128]{2,0,1:T(8,128)(2,1)S(1)} %copy-done.2, f32[4,256,2048]{2,1,0:T(8,128)S(1)} %get-tuple-element.45, f32[4,256]{1,0:T(4,128)S(1)} %broadcast_maximum_fusion, f32[4,2048]{1,0:T(4,128)S(1)} %bitcast.42, f32[4,256]{1,0:T(4,128)S(1)} %bitcast.47, pred[256,2048]{1,0:T(8,128)(4,1)S(1)} %iota_compare_fusion, ...), kind=kOutput, calls=%fused_computation.13 | convolution fusion | flops 549584896 | bytes 11579392 | tf_op jit(solution)/shard_map/cond/branch_0_fun/hqk,khd->hqd/dot_general | solution.py:79
  215.5 0.2 copy.19
  215.8 28.0 %all-gather.14.cloned.1.call-done = bf16[512,1024]{1,0:T(8,128)(2,1)} async-done(((bf16[512,128]{1,0:T(8,128)(2,1)}), bf16[512,1024]{1,0:T(8,128)(2,1)}) %all-gather.14.cloned.1.call-update) | async-done | bytes 1048592 | tf_op jit(solution)/shard_map/all_gather | solution.py:101
  243.8 2.7 fusion.31
  246.5 0.0 reduce-scatter.2.cloned.1.call-update
  246.5 24.0 %reduce-scatter.2.cloned.1.call-done = f32[64,1024]{1,0:T(8,128)} async-done(((f32[256,1024]{1,0:T(8,128)}), f32[64,1024]{1,0:T(8,128)}) %reduce-scatter.2.cloned.1.call-update) | async-done | bytes 262160 | tf_op jit(solution)/shard_map/reduce_scatter | solution.py:28
  270.5 1.1 multiply_reduce_fusion
  271.6 0.0 copy-done
  271.6 1.7 multiply_convert_fusion
  (11 shorter events, 0.2 us)
Async XLA Ops:
  6.5 46.0 %all-gather.8.cloned.1.call-start = ((), (), s32[]{:S(2)}) async-start(), calls=%async_computation.2 | async-start | bytes 1179648 | tf_op jit(solution)/shard_map/all_gather | solution.py:39
  7.3 95.2 %all-gather.6.cloned.1.call-start = ((), (), s32[]{:S(2)}) async-start(), calls=%async_computation.1 | async-start | bytes 2359296 | tf_op jit(solution)/shard_map/all_gather | solution.py:10
  9.0 145.3 %all-gather.10.cloned.1.call-start = ((), (), s32[]{:S(2)}) async-start(), calls=%async_computation.3 | async-start | bytes 2359296 | tf_op jit(solution)/shard_map/all_gather | solution.py:22
  39.2 68.7 %copy-start.1 = (f32[4]{0:T(128)S(1)}, f32[4]{0:T(128)}, u32[]{:S(2)}) copy-start(f32[4]{0:T(128)} %param.15) | copy-start | bytes 52
  106.4 97.6 %all-gather.12.cloned.1.call-start = ((), (), s32[]{:S(2)}) async-start(), calls=%async_computation.4 | async-start | bytes 2359296 | tf_op jit(solution)/shard_map/all_gather | solution.py:22
  107.3 136.5 %all-gather.14.cloned.1.call-start = ((), (), s32[]{:S(2)}) async-start(), calls=%async_computation.5 | async-start | bytes 1179648 | tf_op jit(solution)/shard_map/all_gather | solution.py:101
  107.9 162.6 %reduce-scatter.2.cloned.1.call-start = ((), (), s32[]{:S(2)}) async-start(), calls=%async_computation.6 | async-start | bytes 1310720 | tf_op jit(solution)/shard_map/reduce_scatter | solution.py:28
  204.0 67.6 %copy-start = (f32[1024]{0:T(1024)S(1)}, f32[1024]{0:T(1024)}, u32[]{:S(2)}) copy-start(f32[1024]{0:T(1024)} %param.17) | copy-start | bytes 12292
  204.4 7.9 %copy-start.2 = (bf16[2048,4,128]{2,0,1:T(8,128)(2,1)S(1)}, bf16[2048,4,128]{2,0,1:T(8,128)(2,1)}, u32[]{:S(2)}) copy-start(bf16[2048,4,128]{2,0,1:T(8,128)(2,1)} %get-tuple-element.28) | copy-start | bytes 6291460 | tf_op jit(solution)/shard_map/cond
Sparse Core Ops, SparseCore 0:
  9.5 43.0 all-gather.7
  54.6 47.7 all-gather.5
  106.5 47.7 all-gather.9
  156.3 47.6 all-gather.11
  205.9 37.9 all-gather.13
  246.7 23.7 reduce-scatter.1
